TPU v7x, 32 devices: a whole 2x2x4 slice. The times are simulated.
32 devices in a mesh: sp: 16 (over z, y, x), tp: 2 (over core).
Axes of the slice: x: 2, y: 2, z: 4, core: 2. Of those that a mesh axis runs over, the one named last changes fastest.
Arguments:
- queries: bfloat16 [8192, 2048], P('sp', 'tp'), may hold values from -14 to 14
- key_states: bfloat16 [8192, 512], P('sp', 'tp'), may hold values from -14 to 14
- value_states: bfloat16 [8192, 512], P('sp', 'tp'), may hold values from -6 to 6
- sink_logits: float32 [32], P('tp'), may hold values from 0 to 5
- out_weight: bfloat16 [2048, 2048], P('tp'), may hold values from -0.125 to 0.125
- residual: bfloat16 [8192, 2048], P(('sp', 'tp')), may hold values from -6 to 6
- gain_attn: float32 [2048], replicated, may hold values from 0.1 to 1.9
- gain_before: float32 [2048], replicated, may hold values from 0.1 to 1.9
- gain_after: float32 [2048], replicated, may hold values from 0.1 to 1.9
- gate_weight: bfloat16 [2048, 5632], P('sp', 'tp'), may hold values from -0.125 to 0.125
- value_weight: bfloat16 [2048, 5632], P('sp', 'tp'), may hold values from -0.125 to 0.125
- gate_taps: float32 [3, 5632], P(None, 'tp'), may hold values from -3 to 3
- value_taps: float32 [3, 5632], P(None, 'tp'), may hold values from -3 to 3
- down_weight: bfloat16 [5632, 2048], P('tp', 'sp'), may hold values from -0.078125 to 0.078125
Outputs:
- layer_out: bfloat16 [8192, 2048], P(('sp', 'tp'))
All inputs are finite; a program needn't handle non-finite values.
Results may differ from a plain program's by a relative error of at most 0.018.
Values may be sent and summed in bfloat16 or wider, within the bound.
A program may use at most 128 MiB of HBM per device.

v0:
```python
import functools

import jax
import jax.numpy as jnp
from jax import lax
from jax.experimental import pallas as pl
from jax.experimental.pallas import tpu as pltpu
from jax.sharding import PartitionSpec as P

HD = 64
WINDOW = 128
TEAM = 4


NEG_FILL = -1e30
MESH = pl.DeviceIdType.MESH
VMEM_BYTES = 60 * 1024 * 1024

def passed_along(block, axis, distance):
    devices = range(lax.axis_size(axis))
    route = [(i - distance, i) for i in devices if i - distance in devices]
    return lax.ppermute(block, axis, route)


def rms_scale(matrix):
    return matrix * lax.rsqrt(jnp.mean(matrix * matrix, axis=-1, keepdims=True) + 1e-06)


def attention_local(queries, key_states, value_states, sink_logits):
    length = queries.shape[0]
    blocks = length // WINDOW
    kv_local = key_states.shape[1] // HD
    grouping = queries.shape[1] // key_states.shape[1]
    earlier_keys, earlier_values = passed_along(
        (key_states[length - WINDOW :], value_states[length - WINDOW :]), "sp", 1
    )
    keys_ext = jnp.concatenate([earlier_keys, key_states], axis=0).reshape(
        blocks + 1, WINDOW, kv_local, HD
    )
    values_ext = jnp.concatenate([earlier_values, value_states], axis=0).reshape(
        blocks + 1, WINDOW, kv_local, HD
    )
    key_blocks = jnp.concatenate([keys_ext[:-1], keys_ext[1:]], axis=1)
    value_blocks = jnp.concatenate([values_ext[:-1], values_ext[1:]], axis=1)
    query_blocks = queries.reshape(blocks, WINDOW, kv_local, grouping, HD)
    offset = lax.axis_index("sp") * length
    qpos = (offset + jnp.arange(length, dtype=jnp.int32)).reshape(blocks, WINDOW)
    kpos = jnp.concatenate([qpos - WINDOW, qpos], axis=1)
    visible = (
        (kpos[:, None, :] <= qpos[:, :, None])
        & (qpos[:, :, None] - kpos[:, None, :] < WINDOW)
        & (kpos[:, None, :] >= 0)
    )
    scores = jnp.einsum(
        "nqhgd,nkhd->nhgqk", query_blocks, key_blocks, preferred_element_type=jnp.float32
    ) * HD ** (-0.5)
    scores = jnp.where(visible[:, None, None], scores, NEG_FILL)
    sink_col = sink_logits.reshape(kv_local, grouping)[None, :, :, None]
    top = jnp.maximum(jnp.max(scores, axis=-1), sink_col)
    expo = jnp.exp(scores - top[..., None])
    total = jnp.sum(expo, axis=-1) + jnp.exp(sink_col - top)
    probs = (expo / total[..., None]).astype(jnp.bfloat16)
    result = jnp.einsum(
        "nhgqk,nkhd->nqhgd", probs, value_blocks, preferred_element_type=jnp.float32
    )
    return result.astype(jnp.bfloat16).reshape(length, queries.shape[1])


def causal_local(upward, earlier, kernel):
    length = upward.shape[0]
    padded = jnp.concatenate([earlier, upward], axis=0).astype(jnp.float32)
    result = jnp.zeros(upward.shape, jnp.float32)
    for tap_index in range(kernel.shape[0]):
        result = result + kernel[tap_index][None, :] * padded[tap_index : tap_index + length]
    return result


def on_device_plain(
    queries,
    key_states,
    value_states,
    sink_logits,
    out_weight,
    residual,
    gain_attn,
    gain_before,
    gain_after,
    gate_weight,
    value_weight,
    gate_taps,
    value_taps,
    down_weight,
):
    length = queries.shape[0]
    attended = attention_local(queries, key_states, value_states, sink_logits)
    selected = attended
    attn_proj = lax.psum_scatter(
        jnp.dot(selected, out_weight, preferred_element_type=jnp.float32).astype(jnp.bfloat16),
        "tp",
        scatter_dimension=0,
        tiled=True,
    ).astype(jnp.float32)
    middle = residual.astype(jnp.float32) + rms_scale(attn_proj) * gain_attn
    normed = (rms_scale(middle) * gain_before).astype(jnp.bfloat16)
    whole_rows = lax.all_gather(normed, "tp", axis=0, tiled=True)
    gate_full, value_full = (
        lax.all_gather(gate_weight, "sp", axis=0, tiled=True),
        lax.all_gather(value_weight, "sp", axis=0, tiled=True),
    )
    gate_up = jnp.dot(whole_rows, gate_full, preferred_element_type=jnp.float32).astype(
        jnp.bfloat16
    )
    value_up = jnp.dot(whole_rows, value_full, preferred_element_type=jnp.float32).astype(
        jnp.bfloat16
    )
    reach = gate_taps.shape[0] - 1
    gate_before, value_before = passed_along(
        (gate_up[length - reach :], value_up[length - reach :]), "sp", 1
    )
    gate_conv = causal_local(gate_up, gate_before, gate_taps)
    value_conv = causal_local(value_up, value_before, value_taps)
    hidden = (jax.nn.silu(gate_conv) * value_conv).astype(jnp.bfloat16)
    down_whole = lax.all_gather(down_weight, "sp", axis=1, tiled=True)
    selected = hidden
    down = lax.psum_scatter(
        jnp.dot(selected, down_whole, preferred_element_type=jnp.float32).astype(jnp.bfloat16),
        "tp",
        scatter_dimension=0,
        tiled=True,
    ).astype(jnp.float32)
    return (middle + rms_scale(down) * gain_after).astype(jnp.bfloat16)


def team_peer(place, turn):
    low, high = place % 2, place // 2
    if turn & 1:
        low = 1 - low
    if turn & 2:
        high = 1 - high
    return high * 2 + low


def remote(src, dst, send, recv, **device):
    return pltpu.make_async_remote_copy(
        src_ref=src, dst_ref=dst, send_sem=send, recv_sem=recv, device_id=device, device_id_type=MESH
    )


def greet(devices):
    barrier = pltpu.get_barrier_semaphore()
    for device in devices:
        pl.semaphore_signal(barrier, inc=1, device_id=device, device_id_type=MESH)
    pl.semaphore_wait(barrier, len(devices))


def row_scale(block):
    return lax.rsqrt(jnp.mean(block * block, axis=-1, keepdims=True) + 1e-06)


def front_kernel(
    ring,
    q_ref,
    k_ref,
    v_ref,
    sink_ref,
    ow_ref,
    res_ref,
    ga_ref,
    gb_ref,
    gate_in,
    value_in,
    down_in,
    gate_taps,
    value_taps,
    hid_ref,
    down_all,
    mid_ref,
    rows_all,
    gate_all,
    value_all,
    gate_up,
    value_up,
    k_ext,
    v_ext,
    att,
    snd,
    rcv,
    own,
    nrm,
    halo_s,
    halo_r,
    trade_s,
    trade_r,
    local_sem,
    ring_s,
    ring_r,
    pair_s,
    pair_r,
    rows_s,
    rows_r,
    mate_s,
    mate_r,
    tail_s,
    tail_r,
):
    sp, tp = lax.axis_index("sp"), lax.axis_index("tp")
    members = ring * TEAM
    level, place = sp // TEAM, sp % TEAM
    up = (level + 1) % ring * TEAM + place
    down = (level + ring - 1) % ring * TEAM + place
    after, before = (sp + 1) % members, (sp + members - 1) % members
    mate = 1 - tp
    length = q_ref.shape[0]
    share = length // 2
    deep = gate_in.shape[1]
    units = gate_in.shape[2]
    wide = down_in.shape[1]
    sends = []

    greet(
        [{"sp": level * TEAM + team_peer(place, turn)} for turn in range(1, TEAM)]
        + [{"tp": mate}, {"sp": up}, {"sp": down}, {"sp": after}, {"sp": before}]
    )

    def begin(copy):
        copy.start()
        sends.append(copy)
        return copy

    halos = [
        begin(
            remote(
                ref.at[pl.ds(length - WINDOW, WINDOW)],
                ext.at[pl.ds(0, WINDOW)],
                halo_s.at[i],
                halo_r.at[i],
                sp=after,
            )
        )
        for i, (ref, ext) in enumerate(((k_ref, k_ext), (v_ref, v_ext)))
    ]

    def span(m, ref, start, size):
        if m < 2:
            return ref.at[pl.ds(pl.multiple_of(start * deep, deep), size * deep)]
        return ref.at[:, pl.ds(pl.multiple_of(start * wide, wide), size * wide)]

    def piece(m, member):
        if m < 2:
            return (gate_in, value_in)[m].at[member]
        return down_in.at[pl.ds(pl.multiple_of(member * units, units), units)]

    wholes = (gate_all, value_all, down_all)
    trades, locals_ = [], []
    for m in range(3):
        trades.append(
            [
                begin(
                    remote(
                        piece(m, team_peer(place, turn)),
                        span(m, wholes[m], sp, 1),
                        trade_s.at[m, turn - 1],
                        trade_r.at[m, turn - 1],
                        sp=level * TEAM + team_peer(place, turn),
                    )
                )
                for turn in (3, 1, 2)
            ]
        )
        copy = pltpu.make_async_copy(piece(m, place), span(m, wholes[m], sp, 1), local_sem.at[m])
        copy.start()
        locals_.append(copy)

    last = ring // 2
    ring_copies = {}

    def ring_start(m, step):
        if step == 1:
            locals_[m].wait()
            for copy in trades[m]:
                copy.wait_recv()
        for side, towards in ((0, up), (1, down)):
            if step > 1:
                ring_copies[m, step - 1, side].wait_recv()
            source = (level + ring - (step - 1)) % ring if side == 0 else (level + step - 1) % ring
            if step < last:
                block = span(m, wholes[m], source * TEAM, TEAM)
            else:
                block = span(m, wholes[m], source * TEAM + side * (TEAM // 2), TEAM // 2)
            sems = (ring_s.at[m, step - 1, side], ring_r.at[m, step - 1, side])
            ring_copies[m, step, side] = begin(remote(block, block, *sems, sp=towards))

    k_ext[pl.ds(WINDOW, length)] = k_ref[...]
    v_ext[pl.ds(WINDOW, length)] = v_ref[...]
    for copy in halos:
        copy.wait_recv()
    heads_kv = k_ref.shape[1] // HD
    grouping = q_ref.shape[1] // k_ref.shape[1]
    row = lax.broadcasted_iota(jnp.int32, (WINDOW, 2 * WINDOW), 0)
    col = lax.broadcasted_iota(jnp.int32, (WINDOW, 2 * WINDOW), 1)
    band = (col <= row + WINDOW) & (col > row)

    for kv in range(heads_kv):

        def block_step(n, carry, kv=kv):
            start = pl.multiple_of(n * WINDOW, WINDOW)
            keys = k_ext[pl.ds(start, 2 * WINDOW), kv * HD : (kv + 1) * HD]
            values = v_ext[pl.ds(start, 2 * WINDOW), kv * HD : (kv + 1) * HD]
            wide_q = q_ref[pl.ds(start, WINDOW), kv * grouping * HD : (kv + 1) * grouping * HD]
            visible = band & (col + (sp * length + start - WINDOW) >= 0)
            stacked = jnp.concatenate(
                [wide_q[:, g * HD : (g + 1) * HD] for g in range(grouping)], axis=0
            )
            scores = lax.dot_general(
                stacked, keys, (((1,), (1,)), ((), ())), preferred_element_type=jnp.float32
            ) * HD ** (-0.5)
            probs = []
            for g in range(grouping):
                sink = sink_ref[kv * grouping + g]
                part = jnp.where(visible, scores[g * WINDOW : (g + 1) * WINDOW], NEG_FILL)
                top = jnp.maximum(jnp.max(part, axis=-1, keepdims=True), sink)
                expo = jnp.exp(part - top)
                total = jnp.sum(expo, axis=-1, keepdims=True) + jnp.exp(sink - top)
                probs.append((expo / total).astype(jnp.bfloat16))
            result = jnp.dot(
                jnp.concatenate(probs, axis=0), values, preferred_element_type=jnp.float32
            ).astype(jnp.bfloat16)
            att[pl.ds(start, WINDOW), kv * grouping * HD : (kv + 1) * grouping * HD] = (
                jnp.concatenate(
                    [result[g * WINDOW : (g + 1) * WINDOW] for g in range(grouping)], axis=1
                )
            )
            return carry

        lax.fori_loop(0, length // WINDOW, block_step, 0)
        if kv < 2:
            ring_start(kv, 1)
    for m in range(min(heads_kv, 2), 2):
        ring_start(m, 1)

    columns = ow_ref.shape[1]
    tile = min(512, columns)

    def project(rows_start, target):
        def tile_step(t, carry):
            at = pl.multiple_of(t * tile, tile)
            target[:, pl.ds(at, tile)] = jnp.dot(
                att[pl.ds(rows_start, share)],
                ow_ref[:, pl.ds(at, tile)],
                preferred_element_type=jnp.float32,
            ).astype(jnp.bfloat16)
            return carry

        lax.fori_loop(0, columns // tile, tile_step, 0)

    project(pl.multiple_of(mate * share, share), snd)
    pair = begin(remote(snd, rcv, pair_s, pair_r, tp=mate))
    project(pl.multiple_of(tp * share, share), own)
    pair.wait_recv()
    band_rows = 32

    def norm_step(t, carry):
        at = pl.ds(pl.multiple_of(t * band_rows, band_rows), band_rows)
        proj = own[at].astype(jnp.float32) + rcv[at].astype(jnp.float32)
        middle = res_ref[at].astype(jnp.float32) + proj * row_scale(proj) * ga_ref[...]
        mid_ref[at] = middle
        nrm[at] = (middle * row_scale(middle) * gb_ref[...]).astype(jnp.bfloat16)
        return carry

    lax.fori_loop(0, share // band_rows, norm_step, 0)

    def slot(member, core):
        return rows_all.at[pl.ds(pl.multiple_of((member * 2 + core) * share, share), share)]

    mates = [begin(remote(nrm, slot(place, tp), mate_s.at[0], mate_r.at[0], tp=mate))]
    spread = {
        turn: begin(
            remote(
                nrm,
                slot(place, tp),
                rows_s.at[turn - 1],
                rows_r.at[turn - 1],
                sp=level * TEAM + team_peer(place, turn),
            )
        )
        for turn in (3, 1, 2)
    }
    mine = pltpu.make_async_copy(nrm, slot(place, tp), local_sem.at[3])
    mine.start()
    for step in range(2, last + 1):
        for m in range(2):
            ring_start(m, step)
    ring_start(2, 1)
    for turn in (1, 2, 3):
        spread[turn].wait_recv()
        block = slot(team_peer(place, turn), tp)
        mates.append(begin(remote(block, block, mate_s.at[turn], mate_r.at[turn], tp=mate)))
    mine.wait()
    for copy in mates:
        copy.wait_recv()

    rows = rows_all.shape[0]
    edge = gate_up.shape[0] - rows
    tails = []
    for m, result in enumerate((gate_up, value_up)):
        for side in range(2):
            ring_copies[m, last, side].wait_recv()

        def up_step(t, carry, m=m, result=result):
            at = pl.multiple_of(t * share, share)
            result[pl.ds(pl.multiple_of(at + edge, edge), share)] = jnp.dot(
                rows_all[pl.ds(at, share)], wholes[m][...], preferred_element_type=jnp.float32
            ).astype(jnp.bfloat16)
            return carry

        lax.fori_loop(0, rows // share, up_step, 0)
        tails.append(
            begin(
                remote(
                    result.at[pl.ds(rows, edge)],
                    result.at[pl.ds(0, edge)],
                    tail_s.at[m],
                    tail_r.at[m],
                    sp=up,
                )
            )
        )
    for step in range(2, last + 1):
        ring_start(2, step)
    for tail, result in zip(tails, (gate_up, value_up)):
        tail.wait_recv()
        result[pl.ds(0, edge)] = jnp.where(
            level > 0, result[pl.ds(0, edge)].astype(jnp.float32), 0.0
        ).astype(jnp.bfloat16)
    reach = gate_taps.shape[0] - 1
    conv_rows = 64

    def conv_step(t, carry):
        at = pl.multiple_of(t * conv_rows, conv_rows)

        def mixed(source, taps):
            padded = source[pl.ds(at, conv_rows + edge)].astype(jnp.float32)
            total = jnp.zeros((conv_rows, units), jnp.float32)
            for k in range(reach + 1):
                first = edge - reach + k
                total = total + taps[k : k + 1, :] * padded[first : first + conv_rows]
            return total

        gate = mixed(gate_up, gate_taps)
        value = mixed(value_up, value_taps)
        hid_ref[pl.ds(at, conv_rows)] = (gate / (1.0 + jnp.exp(-gate)) * value).astype(jnp.bfloat16)
        return carry

    lax.fori_loop(0, rows // conv_rows, conv_step, 0)
    for side in range(2):
        ring_copies[2, last, side].wait_recv()
    for copy in sends:
        copy.wait_send()


def back_kernel(
    hid_ref, down_ref, mid_ref, gain_ref, out_ref, psnd, prcv, own, snd, rcv, ps, pr, ts, tr
):
    sp, tp = lax.axis_index("sp"), lax.axis_index("tp")
    level, place = sp // TEAM, sp % TEAM
    mate = 1 - tp
    share = mid_ref.shape[0]
    columns = down_ref.shape[1]
    tile = min(512, columns)
    greet(
        [{"sp": level * TEAM + team_peer(place, turn)} for turn in range(1, TEAM)]
        + [{"tp": mate}]
    )
    order = (3, 1, 2, 0)

    def product(turn, core, store):
        start = pl.multiple_of((team_peer(place, turn) * 2 + core) * share, share)

        def tile_step(t, carry):
            at = pl.ds(pl.multiple_of(t * tile, tile), tile)
            part = jnp.dot(
                hid_ref[pl.ds(start, share)], down_ref[:, at], preferred_element_type=jnp.float32
            )
            store(at, part)
            return carry

        lax.fori_loop(0, columns // tile, tile_step, 0)

    pairs, sends = [], []
    for i, turn in enumerate(order):

        def to_mate(at, part, i=i):
            psnd[i, :, at] = part.astype(jnp.bfloat16)

        product(turn, mate, to_mate)
        copy = remote(psnd.at[i], prcv.at[i], ps.at[i], pr.at[i], tp=mate)
        copy.start()
        pairs.append(copy)
    for i, turn in enumerate(order):
        pairs[i].wait_recv()

        def add_mate(at, part, i=i, turn=turn):
            total = part.astype(jnp.bfloat16).astype(jnp.float32) + prcv[i, :, at].astype(jnp.float32)
            if turn:
                snd[i, :, at] = total.astype(jnp.bfloat16)
            else:
                own[:, at] = total

        product(turn, tp, add_mate)
        if turn:
            copy = remote(
                snd.at[i],
                rcv.at[i],
                ts.at[i],
                tr.at[i],
                sp=level * TEAM + team_peer(place, turn),
            )
            copy.start()
            sends.append(copy)
    for copy in sends:
        copy.wait_recv()
    band_rows = 32

    def norm_step(t, carry):
        at = pl.ds(pl.multiple_of(t * band_rows, band_rows), band_rows)
        total = own[at]
        for i in range(TEAM - 1):
            total = total + rcv[i, at].astype(jnp.float32)
        out_ref[at] = (mid_ref[at] + total * row_scale(total) * gain_ref[...]).astype(out_ref.dtype)
        return carry

    lax.fori_loop(0, share // band_rows, norm_step, 0)
    for copy in pairs + sends:
        copy.wait_send()


def on_device_team(
    ring,
    queries,
    key_states,
    value_states,
    sink_logits,
    out_weight,
    residual,
    gain_attn,
    gain_before,
    gain_after,
    gate_weight,
    value_weight,
    gate_taps,
    value_taps,
    down_weight,
):
    length, width = queries.shape[0], residual.shape[1]
    share = residual.shape[0]
    deep, local_units = gate_weight.shape
    units = local_units // TEAM
    rows = length * TEAM
    vmem = pl.BlockSpec(memory_space=pltpu.VMEM)
    smem = pl.BlockSpec(memory_space=pltpu.SMEM)
    far = pl.BlockSpec(memory_space=pl.ANY)
    dma = pltpu.SemaphoreType.DMA
    bf16, f32 = jnp.bfloat16, jnp.float32

    def by_member(weight):
        return weight.reshape(deep, TEAM, units).transpose(1, 0, 2)

    steps = ring // 2
    first = lax.axis_index("sp") % TEAM * units
    hidden, down_all, middle = pl.pallas_call(
        functools.partial(front_kernel, ring),
        out_shape=(
            jax.ShapeDtypeStruct((rows, units), bf16),
            jax.ShapeDtypeStruct((units, width), bf16),
            jax.ShapeDtypeStruct((share, width), f32),
        ),
        in_specs=[vmem] * 3 + [smem] + [vmem] * 9,
        out_specs=(vmem, far, vmem),
        scratch_shapes=[
            pltpu.VMEM((rows, width), bf16),
            pltpu.VMEM((width, units), bf16),
            pltpu.VMEM((width, units), bf16),
            pltpu.VMEM((rows + 16, units), bf16),
            pltpu.VMEM((rows + 16, units), bf16),
            pltpu.VMEM((length + WINDOW, key_states.shape[1]), bf16),
            pltpu.VMEM((length + WINDOW, key_states.shape[1]), bf16),
            pltpu.VMEM(queries.shape, bf16),
            pltpu.VMEM((share, width), bf16),
            pltpu.VMEM((share, width), bf16),
            pltpu.VMEM((share, width), bf16),
            pltpu.VMEM((share, width), bf16),
            dma((2,)),
            dma((2,)),
            dma((3, TEAM - 1)),
            dma((3, TEAM - 1)),
            dma((4,)),
            dma((3, steps, 2)),
            dma((3, steps, 2)),
            dma(()),
            dma(()),
            dma((TEAM - 1,)),
            dma((TEAM - 1,)),
            dma((TEAM,)),
            dma((TEAM,)),
            dma((2,)),
            dma((2,)),
        ],
        compiler_params=pltpu.CompilerParams(
            collective_id=0, has_side_effects=True, vmem_limit_bytes=VMEM_BYTES
        ),
        name="front",
    )(
        queries,
        key_states,
        value_states,
        sink_logits,
        out_weight,
        residual,
        gain_attn[None],
        gain_before[None],
        by_member(gate_weight),
        by_member(value_weight),
        down_weight,
        lax.dynamic_slice_in_dim(gate_taps, first, units, 1),
        lax.dynamic_slice_in_dim(value_taps, first, units, 1),
    )
    return pl.pallas_call(
        back_kernel,
        out_shape=jax.ShapeDtypeStruct((share, width), bf16),
        in_specs=[vmem] * 4,
        out_specs=vmem,
        scratch_shapes=[
            pltpu.VMEM((TEAM, share, width), bf16),
            pltpu.VMEM((TEAM, share, width), bf16),
            pltpu.VMEM((share, width), f32),
            pltpu.VMEM((TEAM - 1, share, width), bf16),
            pltpu.VMEM((TEAM - 1, share, width), bf16),
            dma((TEAM,)),
            dma((TEAM,)),
            dma((TEAM - 1,)),
            dma((TEAM - 1,)),
        ],
        compiler_params=pltpu.CompilerParams(
            collective_id=1, has_side_effects=True, vmem_limit_bytes=VMEM_BYTES
        ),
        name="back",
    )(hidden, down_all, middle, gain_after[None])


def solution(mesh):
    in_specs = (
        P("sp", "tp"),
        P("sp", "tp"),
        P("sp", "tp"),
        P("tp"),
        P("tp", None),
        P(("sp", "tp"), None),
        P(),
        P(),
        P(),
        P("sp", "tp"),
        P("sp", "tp"),
        P(None, "tp"),
        P(None, "tp"),
        P("tp", "sp"),
    )
    out_specs = P(("sp", "tp"), None)
    members, cores = mesh.shape["sp"], mesh.shape["tp"]
    ring = members // TEAM

    def on_device(*args):
        units, wide = args[13].shape
        teams = cores == 2 and members % TEAM == 0 and ring >= 4 and ring % 2 == 0
        if teams and units % (TEAM * 16) == 0 and wide % 128 == 0:
            return on_device_team(ring, *args)
        return on_device_plain(*args)

    return jax.shard_map(
        on_device, mesh=mesh, in_specs=in_specs, out_specs=out_specs, check_vma=False
    )
```

profile of v0, /device:TPU:0, one launch (start us, length us, event | category | flops | bytes accessed | tf_op | source)
XLA Modules:
  0.0 245.4 jit_solution(10585238750922157842)
XLA Ops:
  0.0 0.0 copy-start
  0.0 1.5 constant_dynamic-slice_fusion
  1.5 1.5 copy.15
  2.9 1.2 copy.16
  4.1 0.0 copy-done
  4.1 0.3 copy.17
  4.5 1.2 copy.18
  5.7 174.0 %front.1 = (bf16[2048,704]{1,0:T(8,128)(2,1)}, bf16[704,2048]{1,0:T(8,128)(2,1)}, f32[256,2048]{1,0:T(8,128)}) custom-call(bf16[512,1024]{1,0:T(8,128)(2,1)} %q_ref.1, bf16[512,256]{1,0:T(8,128)(2,1)} %k_ref.1, bf16[512,256]{1,0:T(8,128)(2,1)} %v_ref.1, f32[16]{0:T(128)} %sink_ref.1, bf16[1024,2048]{1,0:T(8,128)(2,1)} %ow_ref.1, bf16[256,2048]{1,0:T(8,128)(2,1)} %res_ref.1, ...), custom_call_target="tpu_custom_call" | custom-call | tf_op jit(solution)/shard_map/front/pallas_call | solution.py:570
  179.7 63.3 %back.1 = bf16[256,2048]{1,0:T(8,128)(2,1)} custom-call(bf16[2048,704]{1,0:T(8,128)(2,1)} %get-tuple-element.8.hid_ref, bf16[704,2048]{1,0:T(8,128)(2,1)} %get-tuple-element.9.down_ref, f32[256,2048]{1,0:T(8,128)} %get-tuple-element.10.mid_ref, f32[1,2048]{1,0:T(1,128)} %bitcast.13), custom_call_target="tpu_custom_call" | custom-call | tf_op jit(solution)/shard_map/back/pallas_call | solution.py:627
  243.1 2.3 copy.20
Async XLA Ops:
  0.0 4.1 %copy-start = (bf16[128,2816]{1,0:T(8,128)(2,1)S(1)}, bf16[128,2816]{1,0:T(8,128)(2,1)}, u32[]{:S(2)}) copy-start(bf16[128,2816]{1,0:T(8,128)(2,1)} %param.24) | copy-start | bytes 2162692
where the time goes:
time: 246 us; the launch traced here: 245 us
  Pallas kernels  237 us (96%)
  local copies, waits for them, and re-layouts  8.01 us (3%)
    pallas_call x1, Pallas kernels, on_device_team(): pl.pallas_call(functools.partial(front_kernel, ring), out_shape=(jax.Shap...  174 us
    pallas_call x1, Pallas kernels, on_device_team(): pl.pallas_call(back_kernel, out_shape=jax.ShapeDtypeStruct((share, width)...  63.3 us

commit v1 on v0

v1 whole, which is shorter than its diff:
```python
import functools

import jax
import jax.numpy as jnp
from jax import lax
from jax.experimental import pallas as pl
from jax.experimental.pallas import tpu as pltpu
from jax.sharding import PartitionSpec as P

HD = 64
WINDOW = 128
TEAM = 4


NEG_FILL = -1e30
MESH = pl.DeviceIdType.MESH
VMEM_BYTES = 63 * 1024 * 1024

def passed_along(block, axis, distance):
    devices = range(lax.axis_size(axis))
    route = [(i - distance, i) for i in devices if i - distance in devices]
    return lax.ppermute(block, axis, route)


def rms_scale(matrix):
    return matrix * lax.rsqrt(jnp.mean(matrix * matrix, axis=-1, keepdims=True) + 1e-06)


def attention_local(queries, key_states, value_states, sink_logits):
    length = queries.shape[0]
    blocks = length // WINDOW
    kv_local = key_states.shape[1] // HD
    grouping = queries.shape[1] // key_states.shape[1]
    earlier_keys, earlier_values = passed_along(
        (key_states[length - WINDOW :], value_states[length - WINDOW :]), "sp", 1
    )
    keys_ext = jnp.concatenate([earlier_keys, key_states], axis=0).reshape(
        blocks + 1, WINDOW, kv_local, HD
    )
    values_ext = jnp.concatenate([earlier_values, value_states], axis=0).reshape(
        blocks + 1, WINDOW, kv_local, HD
    )
    key_blocks = jnp.concatenate([keys_ext[:-1], keys_ext[1:]], axis=1)
    value_blocks = jnp.concatenate([values_ext[:-1], values_ext[1:]], axis=1)
    query_blocks = queries.reshape(blocks, WINDOW, kv_local, grouping, HD)
    offset = lax.axis_index("sp") * length
    qpos = (offset + jnp.arange(length, dtype=jnp.int32)).reshape(blocks, WINDOW)
    kpos = jnp.concatenate([qpos - WINDOW, qpos], axis=1)
    visible = (
        (kpos[:, None, :] <= qpos[:, :, None])
        & (qpos[:, :, None] - kpos[:, None, :] < WINDOW)
        & (kpos[:, None, :] >= 0)
    )
    scores = jnp.einsum(
        "nqhgd,nkhd->nhgqk", query_blocks, key_blocks, preferred_element_type=jnp.float32
    ) * HD ** (-0.5)
    scores = jnp.where(visible[:, None, None], scores, NEG_FILL)
    sink_col = sink_logits.reshape(kv_local, grouping)[None, :, :, None]
    top = jnp.maximum(jnp.max(scores, axis=-1), sink_col)
    expo = jnp.exp(scores - top[..., None])
    total = jnp.sum(expo, axis=-1) + jnp.exp(sink_col - top)
    probs = (expo / total[..., None]).astype(jnp.bfloat16)
    result = jnp.einsum(
        "nhgqk,nkhd->nqhgd", probs, value_blocks, preferred_element_type=jnp.float32
    )
    return result.astype(jnp.bfloat16).reshape(length, queries.shape[1])


def causal_local(upward, earlier, kernel):
    length = upward.shape[0]
    padded = jnp.concatenate([earlier, upward], axis=0).astype(jnp.float32)
    result = jnp.zeros(upward.shape, jnp.float32)
    for tap_index in range(kernel.shape[0]):
        result = result + kernel[tap_index][None, :] * padded[tap_index : tap_index + length]
    return result


def on_device_plain(
    queries,
    key_states,
    value_states,
    sink_logits,
    out_weight,
    residual,
    gain_attn,
    gain_before,
    gain_after,
    gate_weight,
    value_weight,
    gate_taps,
    value_taps,
    down_weight,
):
    length = queries.shape[0]
    attended = attention_local(queries, key_states, value_states, sink_logits)
    selected = attended
    attn_proj = lax.psum_scatter(
        jnp.dot(selected, out_weight, preferred_element_type=jnp.float32).astype(jnp.bfloat16),
        "tp",
        scatter_dimension=0,
        tiled=True,
    ).astype(jnp.float32)
    middle = residual.astype(jnp.float32) + rms_scale(attn_proj) * gain_attn
    normed = (rms_scale(middle) * gain_before).astype(jnp.bfloat16)
    whole_rows = lax.all_gather(normed, "tp", axis=0, tiled=True)
    gate_full, value_full = (
        lax.all_gather(gate_weight, "sp", axis=0, tiled=True),
        lax.all_gather(value_weight, "sp", axis=0, tiled=True),
    )
    gate_up = jnp.dot(whole_rows, gate_full, preferred_element_type=jnp.float32).astype(
        jnp.bfloat16
    )
    value_up = jnp.dot(whole_rows, value_full, preferred_element_type=jnp.float32).astype(
        jnp.bfloat16
    )
    reach = gate_taps.shape[0] - 1
    gate_before, value_before = passed_along(
        (gate_up[length - reach :], value_up[length - reach :]), "sp", 1
    )
    gate_conv = causal_local(gate_up, gate_before, gate_taps)
    value_conv = causal_local(value_up, value_before, value_taps)
    hidden = (jax.nn.silu(gate_conv) * value_conv).astype(jnp.bfloat16)
    down_whole = lax.all_gather(down_weight, "sp", axis=1, tiled=True)
    selected = hidden
    down = lax.psum_scatter(
        jnp.dot(selected, down_whole, preferred_element_type=jnp.float32).astype(jnp.bfloat16),
        "tp",
        scatter_dimension=0,
        tiled=True,
    ).astype(jnp.float32)
    return (middle + rms_scale(down) * gain_after).astype(jnp.bfloat16)


def team_peer(place, turn):
    low, high = place % 2, place // 2
    if turn & 1:
        low = 1 - low
    if turn & 2:
        high = 1 - high
    return high * 2 + low


def remote(src, dst, send, recv, **device):
    return pltpu.make_async_remote_copy(
        src_ref=src, dst_ref=dst, send_sem=send, recv_sem=recv, device_id=device, device_id_type=MESH
    )


def row_scale(block):
    return lax.rsqrt(jnp.mean(block * block, axis=-1, keepdims=True) + 1e-06)


def rows_by_units(rows, weight):
    return lax.dot_general(
        rows, weight, (((1,), (1,)), ((), ())), preferred_element_type=jnp.float32
    )


def even_parts(total, wanted):
    for parts in range(wanted, 0, -1):
        if total % (parts * 16) == 0:
            return parts


def layer_kernel(
    ring,
    q_ref,
    k_ref,
    v_ref,
    sink_ref,
    ow_far,
    res_far,
    ga_ref,
    gb_ref,
    gc_ref,
    gate_far,
    value_far,
    down_far,
    gate_taps,
    value_taps,
    out_ref,
    ow,
    res,
    mid,
    gate_all,
    value_all,
    down_all,
    rows_all,
    gate_up,
    value_up,
    hid,
    taps,
    k_ext,
    v_ext,
    att,
    snd,
    rcv,
    own,
    psnd,
    prcv,
    mine,
    keep,
    h1s,
    h1r,
    h2s,
    h2r,
    total,
    halo_s,
    halo_r,
    trade_s,
    trade_r,
    local_sem,
    first_s,
    first_r,
    next_s,
    next_r,
    half_s,
    half_r,
    pair_s,
    pair_r,
    rows_s,
    rows_r,
    mate_s,
    mate_r,
    edge_s,
    edge_r,
    sum_s,
    sum_r,
):
    sp, tp = lax.axis_index("sp"), lax.axis_index("tp")
    members = ring * TEAM
    level, place = sp // TEAM, sp % TEAM
    mate = 1 - tp
    length = q_ref.shape[0]
    share = length // 2
    units = gate_all.shape[0]
    wide = gate_far.shape[1]
    last = ring - 2
    sends = []

    def peer(turn):
        return level * TEAM + team_peer(place, turn)

    has_up, has_down = level < ring - 1, level > 0
    has_after, has_before = sp < members - 1, sp > 0

    barrier = pltpu.get_barrier_semaphore()

    def greet(**device):
        pl.semaphore_signal(barrier, inc=1, device_id=device, device_id_type=MESH)

    greet(tp=mate)
    for turn in (1, 2, 3):
        greet(sp=peer(turn))
    pl.when(has_up)(lambda: greet(sp=sp + TEAM))
    pl.when(has_down)(lambda: greet(sp=sp - TEAM))
    pl.when(has_after)(lambda: greet(sp=sp + 1))
    pl.when(has_before)(lambda: greet(sp=sp - 1))
    others = sum(jnp.where(there, 1, 0) for there in (has_up, has_down, has_after, has_before))
    pl.semaphore_wait(barrier, TEAM + others)

    def begin(copy, there=None):
        if there is None:
            copy.start()
        else:
            pl.when(there)(copy.start)
        sends.append((there, copy))
        return copy

    def arrive(copy, there=None):
        if there is None:
            copy.wait_recv()
        else:
            pl.when(there)(copy.wait_recv)

    halos = [
        begin(
            remote(
                ref.at[pl.ds(length - WINDOW, WINDOW)],
                ext.at[pl.ds(0, WINDOW)],
                halo_s.at[i],
                halo_r.at[i],
                sp=sp + 1,
            ),
            has_after,
        )
        for i, (ref, ext) in enumerate(((k_ref, k_ext), (v_ref, v_ext)))
    ]

    fars = (gate_far, value_far, down_far)
    wholes = (gate_all, value_all, down_all)

    def span(m, start, size):
        return wholes[m].at[:, pl.ds(pl.multiple_of(start * wide, wide), size * wide)]

    def piece(m, member):
        return fars[m].at[pl.ds(pl.multiple_of(member * units, units), units)]

    def can_send(side, step):
        return has_up & (level >= step) if side == 0 else has_down & (level + step < ring)

    def can_receive(side, step):
        return level > step if side == 0 else level + step < ring - 1

    def toward(side):
        return sp + TEAM if side == 0 else sp - TEAM

    def first_copy(m, side, q, source=None):
        block = span(m, level * TEAM + q, 1)
        return remote(
            block if source is None else source,
            block,
            first_s.at[m, side, q],
            first_r.at[m, side, q],
            sp=toward(side),
        )

    def next_copy(m, side, step, block, half=None):
        if half is None:
            part = span(m, block * TEAM, TEAM)
            sems = next_s.at[m, side, step - 1], next_r.at[m, side, step - 1]
        else:
            part = span(m, block * TEAM + half * (TEAM // 2), TEAM // 2)
            sems = half_s.at[side, step - 1, half], half_r.at[side, step - 1, half]
        return remote(part, part, *sems, sp=toward(side))

    def came(side, step):
        return level - 1 - step if side == 0 else level + 1 + step

    def receive(m, step, half=None):
        for side in range(2):
            there = can_receive(side, step)
            if step == 0:
                members_in = range(TEAM) if half is None else range(half * 2, half * 2 + 2)
                for q in members_in:
                    block = span(m, came(side, 0) * TEAM + q, 1)
                    sems = first_s.at[m, side, q], first_r.at[m, side, q]
                    arrive(remote(block, block, *sems, sp=toward(side)), there)
            else:
                arrive(next_copy(m, side, step, came(side, step), half), there)

    def pass_on(m, step, half=None):
        receive(m, step - 1, half)
        for side in range(2):
            block = level - step if side == 0 else level + step
            begin(next_copy(m, side, step, block, half), can_send(side, step))

    trades, locals_ = [], []
    for m in range(3):
        trades.append(
            {
                turn: begin(
                    remote(
                        piece(m, team_peer(place, turn)),
                        span(m, sp, 1),
                        trade_s.at[m, turn - 1],
                        trade_r.at[m, turn - 1],
                        sp=peer(turn),
                    )
                )
                for turn in (3, 1, 2)
            }
        )
        for side in range(2):
            begin(first_copy(m, side, place, piece(m, place)), can_send(side, 0))
        copy = pltpu.make_async_copy(piece(m, place), span(m, sp, 1), local_sem.at[m])
        copy.start()
        locals_.append(copy)
    fetch_ow = pltpu.make_async_copy(ow_far, ow, local_sem.at[3])
    fetch_ow.start()
    fetch_res = pltpu.make_async_copy(res_far, res, local_sem.at[4])
    fetch_res.start()

    def first_rest(m):
        for turn in (1, 2, 3):
            trades[m][turn].wait_recv()
            for side in range(2):
                begin(first_copy(m, side, team_peer(place, turn)), can_send(side, 0))

    pending = [(m, step) for step in range(1, last + 1) for m in range(2)]

    def pass_next(count):
        for m, step in pending[:count]:
            pass_on(m, step)
        del pending[:count]

    k_ext[pl.ds(WINDOW, length)] = k_ref[...]
    v_ext[pl.ds(WINDOW, length)] = v_ref[...]

    @pl.when(jnp.logical_not(has_before))
    def _():
        k_ext[pl.ds(0, WINDOW)] = jnp.zeros((WINDOW, k_ref.shape[1]), k_ref.dtype)
        v_ext[pl.ds(0, WINDOW)] = jnp.zeros((WINDOW, k_ref.shape[1]), k_ref.dtype)

    for p in range(TEAM):

        @pl.when(place == p)
        def _(p=p):
            for i, ref in enumerate((gate_taps, value_taps)):
                taps[i, : ref.shape[0]] = ref[:, p * units : (p + 1) * units]

    for copy in halos:
        arrive(copy, has_before)
    heads_kv = k_ref.shape[1] // HD
    grouping = q_ref.shape[1] // k_ref.shape[1]
    row = lax.broadcasted_iota(jnp.int32, (WINDOW, 2 * WINDOW), 0)
    col = lax.broadcasted_iota(jnp.int32, (WINDOW, 2 * WINDOW), 1)
    band = (col <= row + WINDOW) & (col > row)

    for kv in range(heads_kv):

        def block_step(n, carry, kv=kv):
            start = pl.multiple_of(n * WINDOW, WINDOW)
            keys = k_ext[pl.ds(start, 2 * WINDOW), kv * HD : (kv + 1) * HD]
            values = v_ext[pl.ds(start, 2 * WINDOW), kv * HD : (kv + 1) * HD]
            wide_q = q_ref[pl.ds(start, WINDOW), kv * grouping * HD : (kv + 1) * grouping * HD]
            visible = band & (col + (sp * length + start - WINDOW) >= 0)
            stacked = jnp.concatenate(
                [wide_q[:, g * HD : (g + 1) * HD] for g in range(grouping)], axis=0
            )
            scores = lax.dot_general(
                stacked, keys, (((1,), (1,)), ((), ())), preferred_element_type=jnp.float32
            ) * HD ** (-0.5)
            probs = []
            for g in range(grouping):
                sink = sink_ref[kv * grouping + g]
                part = jnp.where(visible, scores[g * WINDOW : (g + 1) * WINDOW], NEG_FILL)
                top = jnp.maximum(jnp.max(part, axis=-1, keepdims=True), sink)
                expo = jnp.exp(part - top)
                whole = jnp.sum(expo, axis=-1, keepdims=True) + jnp.exp(sink - top)
                probs.append((expo / whole).astype(jnp.bfloat16))
            result = jnp.dot(
                jnp.concatenate(probs, axis=0), values, preferred_element_type=jnp.float32
            ).astype(jnp.bfloat16)
            att[pl.ds(start, WINDOW), kv * grouping * HD : (kv + 1) * grouping * HD] = (
                jnp.concatenate(
                    [result[g * WINDOW : (g + 1) * WINDOW] for g in range(grouping)], axis=1
                )
            )
            return carry

        lax.fori_loop(0, length // WINDOW, block_step, 0)
    first_rest(0)

    columns = ow.shape[1]
    tile = min(512, columns)
    fetch_ow.wait()

    def project(rows_start, target):
        def tile_step(t, carry):
            at = pl.multiple_of(t * tile, tile)
            target[:, pl.ds(at, tile)] = jnp.dot(
                att[pl.ds(rows_start, share)],
                ow[:, pl.ds(at, tile)],
                preferred_element_type=jnp.float32,
            ).astype(jnp.bfloat16)
            return carry

        lax.fori_loop(0, columns // tile, tile_step, 0)

    project(pl.multiple_of(mate * share, share), snd)
    pair = begin(remote(snd, rcv, pair_s, pair_r, tp=mate))
    project(pl.multiple_of(tp * share, share), own)
    first_rest(1)
    fetch_res.wait()
    pair.wait_recv()
    band_rows = 32
    rows = length * TEAM
    edge = rows_all.shape[0] - rows

    def row_start(member, core):
        return pl.multiple_of(edge + (member * 2 + core) * share, edge)

    my_rows = row_start(place, tp)

    def norm_step(t, carry):
        at = pl.ds(pl.multiple_of(t * band_rows, band_rows), band_rows)
        proj = own[at].astype(jnp.float32) + rcv[at].astype(jnp.float32)
        middle = res[at].astype(jnp.float32) + proj * row_scale(proj) * ga_ref[...]
        mid[at] = middle
        rows_all[pl.ds(pl.multiple_of(my_rows + t * band_rows, edge), band_rows)] = (
            middle * row_scale(middle) * gb_ref[...]
        ).astype(jnp.bfloat16)
        return carry

    lax.fori_loop(0, share // band_rows, norm_step, 0)

    def slot(member, first=0, size=share):
        start = pl.multiple_of(row_start(member, tp) + first, edge)
        return rows_all.at[pl.ds(start, size)]

    def row_copy(block, i, turn):
        return begin(remote(block, block, rows_s.at[i], rows_r.at[i], sp=peer(turn)))

    def to_mate(block, i):
        return begin(remote(block, block, mate_s.at[i], mate_r.at[i], tp=mate))

    half = share // 2
    mine_rows = slot(place)
    across = [row_copy(mine_rows, 0, 1), row_copy(mine_rows, 1, 2)]
    mates = [to_mate(mine_rows, 0)]
    pass_next(2)
    across[0].wait_recv()
    across.append(row_copy(slot(team_peer(place, 1), 0, half), 2, 2))
    mates.append(to_mate(slot(team_peer(place, 1)), 1))
    across[1].wait_recv()
    across.append(row_copy(slot(team_peer(place, 2), half, half), 3, 1))
    mates.append(to_mate(slot(team_peer(place, 2)), 2))
    pass_next(1)
    across[2].wait_recv()
    across[3].wait_recv()
    mates.append(to_mate(slot(team_peer(place, 3)), 3))
    for copy in mates:
        copy.wait_recv()
    ending = remote(
        rows_all.at[pl.ds(rows, edge)], rows_all.at[pl.ds(0, edge)], edge_s, edge_r, sp=sp + TEAM
    )
    begin(ending, has_up)

    @pl.when(jnp.logical_not(has_down))
    def _():
        rows_all[pl.ds(0, edge)] = jnp.zeros((edge, rows_all.shape[1]), rows_all.dtype)

    pass_next(len(pending))
    arrive(ending, has_down)

    steps = even_parts(rows + edge, 4)
    chunk = (rows + edge) // steps

    def up(m, result):
        receive(m, last)
        locals_[m].wait()

        def up_step(t, carry):
            at = pl.ds(pl.multiple_of(t * chunk, edge), chunk)
            result[at] = rows_by_units(rows_all[at], wholes[m][...]).astype(jnp.bfloat16)
            return carry

        lax.fori_loop(0, steps, up_step, 0)

    up(0, gate_up)
    first_rest(2)
    up(1, value_up)
    reach = gate_taps.shape[0] - 1
    conv_rows = 64
    per = share // conv_rows

    def conv_step(t, carry):
        at = pl.multiple_of(t * conv_rows, conv_rows)

        def mixed(source, i):
            padded = source[pl.ds(at, conv_rows + edge)].astype(jnp.float32)
            result = jnp.zeros((conv_rows, units), jnp.float32)
            for k in range(reach + 1):
                first = edge - reach + k
                result = result + taps[i, k : k + 1, :] * padded[first : first + conv_rows]
            return result

        gate = mixed(gate_up, 0)
        value = mixed(value_up, 1)
        group = t // per
        to = (group % 2 * TEAM + group // 2) * share + t % per * conv_rows
        hid[pl.ds(pl.multiple_of(to, conv_rows), conv_rows)] = (
            gate / (1.0 + jnp.exp(-gate)) * value
        ).astype(jnp.bfloat16)
        return carry

    lax.fori_loop(0, rows // conv_rows, conv_step, 0)

    locals_[2].wait()
    pairs = jnp.minimum(level, ring - 1 - level)

    def block_at(i):
        near = jnp.where(i % 2 == 1, level - (i + 1) // 2, level + i // 2)
        return jnp.where(i <= 2 * pairs, near, jnp.where(level < ring // 2, i, ring - 1 - i))

    group_cols = TEAM // 2 * wide
    jobs = [(i, h) for i in range(ring) for h in range(2)]

    def cols_of(j):
        i, h = jobs[j]
        return pl.ds(
            pl.multiple_of((block_at(i) * TEAM + h * (TEAM // 2)) * wide, group_cols), group_cols
        )

    def turns_of(j):
        return (1, 2) if j % 2 == 0 else (2, 1)

    many = TEAM * share
    half_many = many // 2

    def product(core, cols, store):
        def step(t, carry):
            at = pl.multiple_of(t * half_many, half_many)
            store(
                pl.ds(at, half_many),
                jnp.dot(
                    hid[pl.ds(pl.multiple_of(core * many + at, half_many), half_many)],
                    down_all[:, cols],
                    preferred_element_type=jnp.float32,
                ).astype(jnp.bfloat16),
            )
            return carry

        lax.fori_loop(0, 2, step, 0)

    twos, ones, seconds = {}, {}, {}

    def stage_product(j):
        i, h = jobs[j]
        if i >= 1:
            if i <= last:
                pass_on(2, i, h)
            else:
                receive(2, last, h)
        cols = cols_of(j)

        def away(at, part):
            psnd[j, at] = part

        def here(at, part):
            mine[j % 2, at] = part

        product(mate, cols, away)
        twos[j] = begin(remote(psnd.at[j], prcv.at[j], sum_s.at[0, j], sum_r.at[0, j], tp=mate))
        product(tp, cols, here)

    def shard(j, turn):
        at = pl.ds(pl.multiple_of(team_peer(place, turn) * share, share), share)
        return mine[j % 2, at].astype(jnp.float32) + prcv[j, at].astype(jnp.float32)

    def stage_first(j):
        one, two = turns_of(j)
        twos[j].wait_recv()
        h1s[j, 0] = shard(j, one).astype(jnp.bfloat16)
        h1s[j, 1] = shard(j, 3).astype(jnp.bfloat16)
        ones[j] = begin(
            remote(h1s.at[j], h1r.at[j], sum_s.at[1, j], sum_r.at[1, j], sp=peer(one))
        )
        total[:, cols_of(j)] = shard(j, 0)
        keep[j % 2] = shard(j, two)

    def stage_second(j):
        one, two = turns_of(j)
        ones[j].wait_recv()
        h2s[j] = (keep[j % 2] + h1r[j, 1].astype(jnp.float32)).astype(jnp.bfloat16)
        seconds[j] = begin(
            remote(h2s.at[j], h2r.at[j], sum_s.at[2, j], sum_r.at[2, j], sp=peer(two))
        )
        total[:, cols_of(j)] += h1r[j, 0].astype(jnp.float32)

    def stage_last(j):
        seconds[j].wait_recv()
        total[:, cols_of(j)] += h2r[j].astype(jnp.float32)

    stages = (stage_product, stage_first, stage_second, stage_last)
    for clock in range(len(jobs) + len(stages) - 1):
        for late in reversed(range(len(stages))):
            if 0 <= clock - late < len(jobs):
                stages[late](clock - late)

    def out_step(t, carry):
        at = pl.ds(pl.multiple_of(t * band_rows, band_rows), band_rows)
        block = total[at]
        out_ref[at] = (mid[at] + block * row_scale(block) * gc_ref[...]).astype(out_ref.dtype)
        return carry

    lax.fori_loop(0, share // band_rows, out_step, 0)
    for there, copy in sends:
        if there is None:
            copy.wait_send()
        else:
            pl.when(there)(copy.wait_send)


def on_device_team(
    ring,
    queries,
    key_states,
    value_states,
    sink_logits,
    out_weight,
    residual,
    gain_attn,
    gain_before,
    gain_after,
    gate_weight,
    value_weight,
    gate_taps,
    value_taps,
    down_weight,
):
    length, width = queries.shape[0], residual.shape[1]
    share = residual.shape[0]
    wide, local_units = gate_weight.shape
    units = local_units // TEAM
    rows = length * TEAM
    edge = 16
    vmem = pl.BlockSpec(memory_space=pltpu.VMEM)
    smem = pl.BlockSpec(memory_space=pltpu.SMEM)
    far = pl.BlockSpec(memory_space=pl.ANY)
    dma = pltpu.SemaphoreType.DMA
    bf16, f32 = jnp.bfloat16, jnp.float32
    jobs, group_cols = ring * 2, TEAM // 2 * wide

    def buffer(*shape, dtype=bf16):
        return pltpu.VMEM(shape, dtype)

    return pl.pallas_call(
        functools.partial(layer_kernel, ring),
        out_shape=jax.ShapeDtypeStruct((share, width), bf16),
        in_specs=[vmem] * 3 + [smem] + [far] * 2 + [vmem] * 3 + [far] * 3 + [vmem] * 2,
        out_specs=vmem,
        scratch_shapes=[
            buffer(*out_weight.shape),
            buffer(share, width),
            buffer(share, width, dtype=f32),
            buffer(units, width),
            buffer(units, width),
            buffer(units, width),
            buffer(rows + edge, width),
            buffer(rows + edge, units),
            buffer(rows + edge, units),
            buffer(rows, units),
            buffer(2, 8, units, dtype=f32),
            buffer(length + WINDOW, key_states.shape[1]),
            buffer(length + WINDOW, key_states.shape[1]),
            buffer(*queries.shape),
            buffer(share, width),
            buffer(share, width),
            buffer(share, width),
            buffer(jobs, TEAM * share, group_cols),
            buffer(jobs, TEAM * share, group_cols),
            buffer(2, TEAM * share, group_cols),
            buffer(2, share, group_cols, dtype=f32),
            buffer(jobs, 2, share, group_cols),
            buffer(jobs, 2, share, group_cols),
            buffer(jobs, share, group_cols),
            buffer(jobs, share, group_cols),
            buffer(share, width, dtype=f32),
            dma((2,)),
            dma((2,)),
            dma((3, TEAM - 1)),
            dma((3, TEAM - 1)),
            dma((5,)),
            dma((3, 2, TEAM)),
            dma((3, 2, TEAM)),
            dma((2, 2, ring - 2)),
            dma((2, 2, ring - 2)),
            dma((2, ring - 2, 2)),
            dma((2, ring - 2, 2)),
            dma(()),
            dma(()),
            dma((4,)),
            dma((4,)),
            dma((TEAM,)),
            dma((TEAM,)),
            dma(()),
            dma(()),
            dma((3, jobs)),
            dma((3, jobs)),
        ],
        compiler_params=pltpu.CompilerParams(
            collective_id=0, has_side_effects=True, vmem_limit_bytes=VMEM_BYTES
        ),
        name="layer",
    )(
        queries,
        key_states,
        value_states,
        sink_logits,
        out_weight,
        residual,
        gain_attn[None],
        gain_before[None],
        gain_after[None],
        gate_weight.T,
        value_weight.T,
        down_weight,
        gate_taps,
        value_taps,
    )


def solution(mesh):
    in_specs = (
        P("sp", "tp"),
        P("sp", "tp"),
        P("sp", "tp"),
        P("tp"),
        P("tp", None),
        P(("sp", "tp"), None),
        P(),
        P(),
        P(),
        P("sp", "tp"),
        P("sp", "tp"),
        P(None, "tp"),
        P(None, "tp"),
        P("tp", "sp"),
    )
    out_specs = P(("sp", "tp"), None)
    members, cores = mesh.shape["sp"], mesh.shape["tp"]
    ring = members // TEAM

    def on_device(*args):
        units, wide = args[13].shape
        teams = cores == 2 and members % TEAM == 0 and ring >= 3
        if teams and units % (TEAM * 16) == 0 and wide % 128 == 0:
            return on_device_team(ring, *args)
        return on_device_plain(*args)

    return jax.shard_map(
        on_device, mesh=mesh, in_specs=in_specs, out_specs=out_specs, check_vma=False
    )
```

time: 246 us -> 214 us (0.87)
  Pallas kernels: 237 us -> 207 us
    pallas_call x2 -> x1, Pallas kernels: 237 us -> 207 us  [on_device_team(): pl.pallas_call(functools.partial(layer_kernel, ring), out_shape=jax.Shape...]
    unnamed x5 -> x3, local copies, waits for them, and re-layouts: 4.11 us -> 6.81 us
where the time goes in v1:
time: 214 us
  Pallas kernels  207 us (97%)
  local copies, waits for them, and re-layouts  6.81 us (3%)
    pallas_call x1, Pallas kernels, on_device_team(): pl.pallas_call(functools.partial(layer_kernel, ring), out_shape=jax.Shape...  207 us
    unnamed x3, local copies, waits for them, and re-layouts  6.81 us

profile of v1, /device:TPU:0, one launch (start us, length us, event | category | flops | bytes accessed | tf_op | source)
XLA Modules:
  0.0 214.1 jit_solution(10279806323776059191)
XLA Ops:
  0.0 2.2 %copy.15 = bf16[128,2816]{0,1:T(8,128)(2,1)} copy(bf16[128,2816]{1,0:T(8,128)(2,1)} %param.23) | data formatting | bytes 1441792 | tf_op args[9]
  2.2 2.3 %copy.16 = bf16[128,2816]{0,1:T(8,128)(2,1)} copy(bf16[128,2816]{1,0:T(8,128)(2,1)} %param.24) | data formatting | bytes 1441792 | tf_op args[10]
  4.5 207.3 %layer.1 = bf16[256,2048]{1,0:T(8,128)(2,1)} custom-call(bf16[512,1024]{1,0:T(8,128)(2,1)} %q_ref.1, bf16[512,256]{1,0:T(8,128)(2,1)} %k_ref.1, bf16[512,256]{1,0:T(8,128)(2,1)} %v_ref.1, f32[16]{0:T(128)} %sink_ref.1, bf16[1024,2048]{1,0:T(8,128)(2,1)} %ow_far.1, bf16[256,2048]{1,0:T(8,128)(2,1)} %res_far.1, f32[1,2048]{1,0:T(1,128)} %bitcast.7, ...), custom_call_target="tpu_custom_call" | custom-call | tf_op jit(solution)/shard_map/layer/pallas_call | solution.py:709
  211.8 2.3 %copy.18 = bf16[256,2048]{1,0:T(8,128)(2,1)} copy(bf16[256,2048]{1,0:T(8,128)(2,1)} %layer.1) | data formatting | bytes 2097152

commit v2 on v1

--- a/solution.py
+++ b/solution.py
@@ -583,8 +583,12 @@
             pl.multiple_of((block_at(i) * TEAM + h * (TEAM // 2)) * wide, group_cols), group_cols
         )
 
-    def turns_of(j):
-        return (1, 2) if j % 2 == 0 else (2, 1)
+    ways = ((1, 2), (2, 1))
+
+    def part_of(j, way):
+        i, h = jobs[j]
+        first = (block_at(i) * TEAM + h * (TEAM // 2)) * wide + way * wide
+        return pl.ds(pl.multiple_of(first, wide), wide)
 
     many = TEAM * share
     half_many = many // 2
@@ -625,39 +629,42 @@
         twos[j] = begin(remote(psnd.at[j], prcv.at[j], sum_s.at[0, j], sum_r.at[0, j], tp=mate))
         product(tp, cols, here)
 
-    def shard(j, turn):
+    def shard(j, way, turn):
         at = pl.ds(pl.multiple_of(team_peer(place, turn) * share, share), share)
-        return mine[j % 2, at].astype(jnp.float32) + prcv[j, at].astype(jnp.float32)
+        cols = pl.ds(way * wide, wide)
+        return mine[j % 2, at, cols].astype(jnp.float32) + prcv[j, at, cols].astype(jnp.float32)
 
     def stage_first(j):
-        one, two = turns_of(j)
         twos[j].wait_recv()
-        h1s[j, 0] = shard(j, one).astype(jnp.bfloat16)
-        h1s[j, 1] = shard(j, 3).astype(jnp.bfloat16)
-        ones[j] = begin(
-            remote(h1s.at[j], h1r.at[j], sum_s.at[1, j], sum_r.at[1, j], sp=peer(one))
-        )
-        total[:, cols_of(j)] = shard(j, 0)
-        keep[j % 2] = shard(j, two)
+        for way, (one, two) in enumerate(ways):
+            h1s[j, way, 0] = shard(j, way, one).astype(jnp.bfloat16)
+            h1s[j, way, 1] = shard(j, way, 3).astype(jnp.bfloat16)
+            sems = sum_s.at[1 + way, j], sum_r.at[1 + way, j]
+            ones[j, way] = begin(remote(h1s.at[j, way], h1r.at[j, way], *sems, sp=peer(one)))
+        for way, (one, two) in enumerate(ways):
+            total[:, part_of(j, way)] = shard(j, way, 0)
+            keep[j % 4, way] = shard(j, way, two)
 
     def stage_second(j):
-        one, two = turns_of(j)
-        ones[j].wait_recv()
-        h2s[j] = (keep[j % 2] + h1r[j, 1].astype(jnp.float32)).astype(jnp.bfloat16)
-        seconds[j] = begin(
-            remote(h2s.at[j], h2r.at[j], sum_s.at[2, j], sum_r.at[2, j], sp=peer(two))
-        )
-        total[:, cols_of(j)] += h1r[j, 0].astype(jnp.float32)
+        for way, (one, two) in enumerate(ways):
+            ones[j, way].wait_recv()
+            h2s[j, way] = (keep[j % 4, way] + h1r[j, way, 1].astype(jnp.float32)).astype(
+                jnp.bfloat16
+            )
+            sems = sum_s.at[3 + way, j], sum_r.at[3 + way, j]
+            seconds[j, way] = begin(remote(h2s.at[j, way], h2r.at[j, way], *sems, sp=peer(two)))
+            total[:, part_of(j, way)] += h1r[j, way, 0].astype(jnp.float32)
 
     def stage_last(j):
-        seconds[j].wait_recv()
-        total[:, cols_of(j)] += h2r[j].astype(jnp.float32)
-
-    stages = (stage_product, stage_first, stage_second, stage_last)
-    for clock in range(len(jobs) + len(stages) - 1):
-        for late in reversed(range(len(stages))):
+        for way in range(2):
+            seconds[j, way].wait_recv()
+            total[:, part_of(j, way)] += h2r[j, way].astype(jnp.float32)
+
+    stages = ((stage_last, 5), (stage_second, 3), (stage_first, 1), (stage_product, 0))
+    for clock in range(len(jobs) + stages[0][1]):
+        for stage, late in stages:
             if 0 <= clock - late < len(jobs):
-                stages[late](clock - late)
+                stage(clock - late)
 
     def out_step(t, carry):
         at = pl.ds(pl.multiple_of(t * band_rows, band_rows), band_rows)
@@ -732,11 +739,11 @@
             buffer(jobs, TEAM * share, group_cols),
             buffer(jobs, TEAM * share, group_cols),
             buffer(2, TEAM * share, group_cols),
-            buffer(2, share, group_cols, dtype=f32),
-            buffer(jobs, 2, share, group_cols),
-            buffer(jobs, 2, share, group_cols),
-            buffer(jobs, share, group_cols),
-            buffer(jobs, share, group_cols),
+            buffer(4, 2, share, wide, dtype=f32),
+            buffer(jobs, 2, 2, share, wide),
+            buffer(jobs, 2, 2, share, wide),
+            buffer(jobs, 2, share, wide),
+            buffer(jobs, 2, share, wide),
             buffer(share, width, dtype=f32),
             dma((2,)),
             dma((2,)),
@@ -757,8 +764,8 @@
             dma((TEAM,)),
             dma(()),
             dma(()),
-            dma((3, jobs)),
-            dma((3, jobs)),
+            dma((5, jobs)),
+            dma((5, jobs)),
         ],
         compiler_params=pltpu.CompilerParams(
             collective_id=0, has_side_effects=True, vmem_limit_bytes=VMEM_BYTES

time: 214 us -> 177 us (0.83)
  Pallas kernels: 207 us -> 170 us
    pallas_call x1, Pallas kernels: 207 us -> 170 us  [on_device_team(): pl.pallas_call(functools.partial(layer_kernel, ring), out_shape=jax.Shape...]
where the time goes in v2:
time: 177 us; the launch traced here: 176 us
  Pallas kernels  170 us (96%)
  local copies, waits for them, and re-layouts  6.81 us (4%)
    pallas_call x1, Pallas kernels, on_device_team(): pl.pallas_call(functools.partial(layer_kernel, ring), out_shape=jax.Shape...  170 us
    unnamed x3, local copies, waits for them, and re-layouts  6.81 us

profile of v2, /device:TPU:0, one launch (start us, length us, event | category | flops | bytes accessed | tf_op | source)
XLA Modules:
  0.0 176.5 jit_solution(13914904311888566268)
XLA Ops:
  0.0 2.2 %copy.15 = bf16[128,2816]{0,1:T(8,128)(2,1)} copy(bf16[128,2816]{1,0:T(8,128)(2,1)} %param.23) | data formatting | bytes 1441792 | tf_op args[9]
  2.2 2.3 %copy.16 = bf16[128,2816]{0,1:T(8,128)(2,1)} copy(bf16[128,2816]{1,0:T(8,128)(2,1)} %param.24) | data formatting | bytes 1441792 | tf_op args[10]
  4.5 169.7 %layer.1 = bf16[256,2048]{1,0:T(8,128)(2,1)} custom-call(bf16[512,1024]{1,0:T(8,128)(2,1)} %q_ref.1, bf16[512,256]{1,0:T(8,128)(2,1)} %k_ref.1, bf16[512,256]{1,0:T(8,128)(2,1)} %v_ref.1, f32[16]{0:T(128)} %sink_ref.1, bf16[1024,2048]{1,0:T(8,128)(2,1)} %ow_far.1, bf16[256,2048]{1,0:T(8,128)(2,1)} %res_far.1, f32[1,2048]{1,0:T(1,128)} %bitcast.7, ...), custom_call_target="tpu_custom_call" | custom-call | tf_op jit(solution)/shard_map/layer/pallas_call | solution.py:716
  174.2 2.3 %copy.18 = bf16[256,2048]{1,0:T(8,128)(2,1)} copy(bf16[256,2048]{1,0:T(8,128)(2,1)} %layer.1) | data formatting | bytes 2097152

commit v3 on v2

--- a/solution.py
+++ b/solution.py
@@ -162,9 +162,13 @@
             return parts
 
 
+def unit_parts(units):
+    return [(first, min(256, units - first)) for first in range(0, units, 256)]
+
+
 def layer_kernel(
     ring,
-    q_ref,
+    q_far,
     k_ref,
     v_ref,
     sink_ref,
@@ -179,6 +183,7 @@
     gate_taps,
     value_taps,
     out_ref,
+    q_ref,
     ow,
     res,
     mid,
@@ -236,6 +241,8 @@
     units = gate_all.shape[0]
     wide = gate_far.shape[1]
     last = ring - 2
+    parts = unit_parts(units)
+    cuts = ((0, 2), (2, 1), (3, 1))
     sends = []
 
     def peer(turn):
@@ -316,11 +323,16 @@
         )
 
     def next_copy(m, side, step, block, half=None):
-        if half is None:
+        if m == 0:
             part = span(m, block * TEAM, TEAM)
-            sems = next_s.at[m, side, step - 1], next_r.at[m, side, step - 1]
+            sems = next_s.at[0, side, step - 1], next_r.at[0, side, step - 1]
+        elif m == 1:
+            first, size = parts[half]
+            part = span(m, block * TEAM, TEAM).at[pl.ds(first, size)]
+            sems = next_s.at[1 + half, side, step - 1], next_r.at[1 + half, side, step - 1]
         else:
-            part = span(m, block * TEAM + half * (TEAM // 2), TEAM // 2)
+            first, size = cuts[half]
+            part = span(m, block * TEAM + first, size)
             sems = half_s.at[side, step - 1, half], half_r.at[side, step - 1, half]
         return remote(part, part, *sems, sp=toward(side))
 
@@ -331,7 +343,9 @@
         for side in range(2):
             there = can_receive(side, step)
             if step == 0:
-                members_in = range(TEAM) if half is None else range(half * 2, half * 2 + 2)
+                members_in = range(TEAM)
+                if m == 2:
+                    members_in = range(cuts[half][0], sum(cuts[half]))
                 for q in members_in:
                     block = span(m, came(side, 0) * TEAM + q, 1)
                     sems = first_s.at[m, side, q], first_r.at[m, side, q]
@@ -340,10 +354,15 @@
                 arrive(next_copy(m, side, step, came(side, step), half), there)
 
     def pass_on(m, step, half=None):
-        receive(m, step - 1, half)
+        if not (m == 1 and step == 1 and half):
+            receive(m, step - 1, half)
         for side in range(2):
             block = level - step if side == 0 else level + step
             begin(next_copy(m, side, step, block, half), can_send(side, step))
+
+    def own_first(m):
+        for side in range(2):
+            begin(first_copy(m, side, place, piece(m, place)), can_send(side, 0))
 
     trades, locals_ = [], []
     for m in range(3):
@@ -358,14 +377,21 @@
                         sp=peer(turn),
                     )
                 )
-                for turn in (3, 1, 2)
+                for turn in (1, 2, 3)
             }
         )
-        for side in range(2):
-            begin(first_copy(m, side, place, piece(m, place)), can_send(side, 0))
+        own_first(m)
         copy = pltpu.make_async_copy(piece(m, place), span(m, sp, 1), local_sem.at[m])
         copy.start()
         locals_.append(copy)
+    fetch_q = pltpu.make_async_copy(q_far, q_ref, local_sem.at[5])
+    fetch_q.start()
+    fetch_kv = [
+        pltpu.make_async_copy(ref, ext.at[pl.ds(WINDOW, length)], local_sem.at[6 + i])
+        for i, (ref, ext) in enumerate(((k_ref, k_ext), (v_ref, v_ext)))
+    ]
+    for copy in fetch_kv:
+        copy.start()
     fetch_ow = pltpu.make_async_copy(ow_far, ow, local_sem.at[3])
     fetch_ow.start()
     fetch_res = pltpu.make_async_copy(res_far, res, local_sem.at[4])
@@ -377,15 +403,30 @@
             for side in range(2):
                 begin(first_copy(m, side, team_peer(place, turn)), can_send(side, 0))
 
-    pending = [(m, step) for step in range(1, last + 1) for m in range(2)]
+    def down_rest():
+        for q in range(TEAM):
+            turn = jnp.abs(place % 2 - q % 2) + 2 * jnp.abs(place // 2 - q // 2)
+
+            @pl.when(turn > 0)
+            def _(q=q, turn=turn):
+                block = span(2, level * TEAM + q, 1)
+                sems = trade_s.at[2, turn - 1], trade_r.at[2, turn - 1]
+                remote(block, block, *sems, sp=level * TEAM + q).wait_recv()
+
+            for side in range(2):
+                begin(first_copy(2, side, q), can_send(side, 0) & (turn > 0))
+
+    pending = [
+        (m, step, part)
+        for step in range(1, last + 1)
+        for m in range(2)
+        for part in (range(len(parts)) if m else (None,))
+    ]
 
     def pass_next(count):
-        for m, step in pending[:count]:
-            pass_on(m, step)
+        for m, step, part in pending[:count]:
+            pass_on(m, step, part)
         del pending[:count]
-
-    k_ext[pl.ds(WINDOW, length)] = k_ref[...]
-    v_ext[pl.ds(WINDOW, length)] = v_ref[...]
 
     @pl.when(jnp.logical_not(has_before))
     def _():
@@ -399,8 +440,12 @@
             for i, ref in enumerate((gate_taps, value_taps)):
                 taps[i, : ref.shape[0]] = ref[:, p * units : (p + 1) * units]
 
+    first_rest(0)
     for copy in halos:
         arrive(copy, has_before)
+    fetch_q.wait()
+    for copy in fetch_kv:
+        copy.wait()
     heads_kv = k_ref.shape[1] // HD
     grouping = q_ref.shape[1] // k_ref.shape[1]
     row = lax.broadcasted_iota(jnp.int32, (WINDOW, 2 * WINDOW), 0)
@@ -440,7 +485,8 @@
             return carry
 
         lax.fori_loop(0, length // WINDOW, block_step, 0)
-    first_rest(0)
+        if kv == 0:
+            first_rest(1)
 
     columns = ow.shape[1]
     tile = min(512, columns)
@@ -461,7 +507,6 @@
     project(pl.multiple_of(mate * share, share), snd)
     pair = begin(remote(snd, rcv, pair_s, pair_r, tp=mate))
     project(pl.multiple_of(tp * share, share), own)
-    first_rest(1)
     fetch_res.wait()
     pair.wait_recv()
     band_rows = 32
@@ -499,7 +544,8 @@
     mine_rows = slot(place)
     across = [row_copy(mine_rows, 0, 1), row_copy(mine_rows, 1, 2)]
     mates = [to_mate(mine_rows, 0)]
-    pass_next(2)
+    pass_next(1)
+    pass_next(len(parts))
     across[0].wait_recv()
     across.append(row_copy(slot(team_peer(place, 1), 0, half), 2, 2))
     mates.append(to_mate(slot(team_peer(place, 1)), 1))
@@ -527,45 +573,51 @@
     steps = even_parts(rows + edge, 4)
     chunk = (rows + edge) // steps
 
-    def up(m, result):
-        receive(m, last)
-        locals_[m].wait()
-
+    def up(m, result, first=0, size=units):
         def up_step(t, carry):
             at = pl.ds(pl.multiple_of(t * chunk, edge), chunk)
-            result[at] = rows_by_units(rows_all[at], wholes[m][...]).astype(jnp.bfloat16)
+            result[at, first : first + size] = rows_by_units(
+                rows_all[at], wholes[m][first : first + size]
+            ).astype(jnp.bfloat16)
             return carry
 
         lax.fori_loop(0, steps, up_step, 0)
 
+    receive(0, last)
+    locals_[0].wait()
     up(0, gate_up)
-    first_rest(2)
-    up(1, value_up)
+    down_rest()
+    locals_[1].wait()
     reach = gate_taps.shape[0] - 1
     conv_rows = 64
     per = share // conv_rows
 
-    def conv_step(t, carry):
+    def conv_step(t, carry, first_unit, size):
+        unit_span = slice(first_unit, first_unit + size)
         at = pl.multiple_of(t * conv_rows, conv_rows)
 
         def mixed(source, i):
-            padded = source[pl.ds(at, conv_rows + edge)].astype(jnp.float32)
-            result = jnp.zeros((conv_rows, units), jnp.float32)
+            padded = source[pl.ds(at, conv_rows + edge), unit_span].astype(jnp.float32)
+            result = jnp.zeros((conv_rows, size), jnp.float32)
             for k in range(reach + 1):
                 first = edge - reach + k
-                result = result + taps[i, k : k + 1, :] * padded[first : first + conv_rows]
+                result = result + taps[i, k : k + 1, unit_span] * padded[first : first + conv_rows]
             return result
 
         gate = mixed(gate_up, 0)
         value = mixed(value_up, 1)
         group = t // per
         to = (group % 2 * TEAM + group // 2) * share + t % per * conv_rows
-        hid[pl.ds(pl.multiple_of(to, conv_rows), conv_rows)] = (
+        hid[pl.ds(pl.multiple_of(to, conv_rows), conv_rows), unit_span] = (
             gate / (1.0 + jnp.exp(-gate)) * value
         ).astype(jnp.bfloat16)
         return carry
 
-    lax.fori_loop(0, rows // conv_rows, conv_step, 0)
+    for i, (first_unit, size) in enumerate(parts):
+        receive(1, last, i)
+        up(1, value_up, first_unit, size)
+        mixing = functools.partial(conv_step, first_unit=first_unit, size=size)
+        lax.fori_loop(0, rows // conv_rows, mixing, 0)
 
     locals_[2].wait()
     pairs = jnp.minimum(level, ring - 1 - level)
@@ -574,21 +626,21 @@
         near = jnp.where(i % 2 == 1, level - (i + 1) // 2, level + i // 2)
         return jnp.where(i <= 2 * pairs, near, jnp.where(level < ring // 2, i, ring - 1 - i))
 
-    group_cols = TEAM // 2 * wide
-    jobs = [(i, h) for i in range(ring) for h in range(2)]
+    jobs = [(i, *job) for i in range(ring - 1) for job in ((0, 2, (0,)), (2, 2, (1, 2)))]
+    jobs += [(ring - 1, *cut, (i,)) for i, cut in enumerate(cuts)]
 
     def cols_of(j):
-        i, h = jobs[j]
-        return pl.ds(
-            pl.multiple_of((block_at(i) * TEAM + h * (TEAM // 2)) * wide, group_cols), group_cols
-        )
+        i, first, size, _ = jobs[j]
+        at = pl.multiple_of((block_at(i) * TEAM + first) * wide, size * wide)
+        return pl.ds(at, size * wide)
+
+    def width_of(j):
+        return slice(0, jobs[j][2] * wide)
 
     ways = ((1, 2), (2, 1))
 
-    def part_of(j, way):
-        i, h = jobs[j]
-        first = (block_at(i) * TEAM + h * (TEAM // 2)) * wide + way * wide
-        return pl.ds(pl.multiple_of(first, wide), wide)
+    def part_of(way):
+        return slice(way * half, (way + 1) * half)
 
     many = TEAM * share
     half_many = many // 2
@@ -611,54 +663,62 @@
     twos, ones, seconds = {}, {}, {}
 
     def stage_product(j):
-        i, h = jobs[j]
+        i, needed = jobs[j][0], jobs[j][3]
         if i >= 1:
-            if i <= last:
-                pass_on(2, i, h)
-            else:
-                receive(2, last, h)
+            for cut in needed:
+                if i <= last:
+                    pass_on(2, i, cut)
+                else:
+                    receive(2, last, cut)
         cols = cols_of(j)
 
         def away(at, part):
-            psnd[j, at] = part
+            psnd[j, at, width_of(j)] = part
 
         def here(at, part):
-            mine[j % 2, at] = part
+            mine[j % 2, at, width_of(j)] = part
 
         product(mate, cols, away)
-        twos[j] = begin(remote(psnd.at[j], prcv.at[j], sum_s.at[0, j], sum_r.at[0, j], tp=mate))
+        there = (j, slice(None), width_of(j))
+        sems = sum_s.at[0, j], sum_r.at[0, j]
+        twos[j] = begin(remote(psnd.at[*there], prcv.at[*there], *sems, tp=mate))
         product(tp, cols, here)
 
     def shard(j, way, turn):
-        at = pl.ds(pl.multiple_of(team_peer(place, turn) * share, share), share)
-        cols = pl.ds(way * wide, wide)
+        at = pl.ds(pl.multiple_of(team_peer(place, turn) * share + way * half, half), half)
+        cols = width_of(j)
         return mine[j % 2, at, cols].astype(jnp.float32) + prcv[j, at, cols].astype(jnp.float32)
 
     def stage_first(j):
         twos[j].wait_recv()
+        cols = width_of(j)
         for way, (one, two) in enumerate(ways):
-            h1s[j, way, 0] = shard(j, way, one).astype(jnp.bfloat16)
-            h1s[j, way, 1] = shard(j, way, 3).astype(jnp.bfloat16)
+            h1s[j, way, 0, :, cols] = shard(j, way, one).astype(jnp.bfloat16)
+            h1s[j, way, 1, :, cols] = shard(j, way, 3).astype(jnp.bfloat16)
+            there = (j, way, slice(None), slice(None), cols)
             sems = sum_s.at[1 + way, j], sum_r.at[1 + way, j]
-            ones[j, way] = begin(remote(h1s.at[j, way], h1r.at[j, way], *sems, sp=peer(one)))
+            ones[j, way] = begin(remote(h1s.at[*there], h1r.at[*there], *sems, sp=peer(one)))
         for way, (one, two) in enumerate(ways):
-            total[:, part_of(j, way)] = shard(j, way, 0)
-            keep[j % 4, way] = shard(j, way, two)
+            total[part_of(way), cols_of(j)] = shard(j, way, 0)
+            keep[j % 4, way, :, cols] = shard(j, way, two)
 
     def stage_second(j):
+        cols = width_of(j)
         for way, (one, two) in enumerate(ways):
             ones[j, way].wait_recv()
-            h2s[j, way] = (keep[j % 4, way] + h1r[j, way, 1].astype(jnp.float32)).astype(
-                jnp.bfloat16
-            )
+            h2s[j, way, :, cols] = (
+                keep[j % 4, way, :, cols] + h1r[j, way, 1, :, cols].astype(jnp.float32)
+            ).astype(jnp.bfloat16)
+            there = (j, way, slice(None), cols)
             sems = sum_s.at[3 + way, j], sum_r.at[3 + way, j]
-            seconds[j, way] = begin(remote(h2s.at[j, way], h2r.at[j, way], *sems, sp=peer(two)))
-            total[:, part_of(j, way)] += h1r[j, way, 0].astype(jnp.float32)
+            seconds[j, way] = begin(remote(h2s.at[*there], h2r.at[*there], *sems, sp=peer(two)))
+            total[part_of(way), cols_of(j)] += h1r[j, way, 0, :, cols].astype(jnp.float32)
 
     def stage_last(j):
+        cols = width_of(j)
         for way in range(2):
             seconds[j, way].wait_recv()
-            total[:, part_of(j, way)] += h2r[j, way].astype(jnp.float32)
+            total[part_of(way), cols_of(j)] += h2r[j, way, :, cols].astype(jnp.float32)
 
     stages = ((stage_last, 5), (stage_second, 3), (stage_first, 1), (stage_product, 0))
     for clock in range(len(jobs) + stages[0][1]):
@@ -708,7 +768,7 @@
     far = pl.BlockSpec(memory_space=pl.ANY)
     dma = pltpu.SemaphoreType.DMA
     bf16, f32 = jnp.bfloat16, jnp.float32
-    jobs, group_cols = ring * 2, TEAM // 2 * wide
+    jobs, group_cols = ring * 2 + 1, TEAM // 2 * wide
 
     def buffer(*shape, dtype=bf16):
         return pltpu.VMEM(shape, dtype)
@@ -716,9 +776,10 @@
     return pl.pallas_call(
         functools.partial(layer_kernel, ring),
         out_shape=jax.ShapeDtypeStruct((share, width), bf16),
-        in_specs=[vmem] * 3 + [smem] + [far] * 2 + [vmem] * 3 + [far] * 3 + [vmem] * 2,
+        in_specs=[far] * 3 + [smem] + [far] * 2 + [vmem] * 3 + [far] * 3 + [vmem] * 2,
         out_specs=vmem,
         scratch_shapes=[
+            buffer(*queries.shape),
             buffer(*out_weight.shape),
             buffer(share, width),
             buffer(share, width, dtype=f32),
@@ -739,23 +800,23 @@
             buffer(jobs, TEAM * share, group_cols),
             buffer(jobs, TEAM * share, group_cols),
             buffer(2, TEAM * share, group_cols),
-            buffer(4, 2, share, wide, dtype=f32),
-            buffer(jobs, 2, 2, share, wide),
-            buffer(jobs, 2, 2, share, wide),
-            buffer(jobs, 2, share, wide),
-            buffer(jobs, 2, share, wide),
+            buffer(4, 2, share // 2, group_cols, dtype=f32),
+            buffer(jobs, 2, 2, share // 2, group_cols),
+            buffer(jobs, 2, 2, share // 2, group_cols),
+            buffer(jobs, 2, share // 2, group_cols),
+            buffer(jobs, 2, share // 2, group_cols),
             buffer(share, width, dtype=f32),
             dma((2,)),
             dma((2,)),
             dma((3, TEAM - 1)),
             dma((3, TEAM - 1)),
-            dma((5,)),
+            dma((8,)),
             dma((3, 2, TEAM)),
             dma((3, 2, TEAM)),
-            dma((2, 2, ring - 2)),
-            dma((2, 2, ring - 2)),
-            dma((2, ring - 2, 2)),
-            dma((2, ring - 2, 2)),
+            dma((1 + len(unit_parts(units)), 2, ring - 2)),
+            dma((1 + len(unit_parts(units)), 2, ring - 2)),
+            dma((2, ring - 2, 3)),
+            dma((2, ring - 2, 3)),
             dma(()),
             dma(()),
             dma((4,)),

time: 177 us -> 170 us (0.960)
  Pallas kernels: 170 us -> 163 us
    pallas_call x1, Pallas kernels: 170 us -> 163 us  [on_device_team(): pl.pallas_call(functools.partial(layer_kernel, ring), out_shape=jax.Shape...]
where the time goes in v3:
time: 170 us
  Pallas kernels  163 us (96%)
  local copies, waits for them, and re-layouts  6.81 us (4%)
    pallas_call x1, Pallas kernels, on_device_team(): pl.pallas_call(functools.partial(layer_kernel, ring), out_shape=jax.Shape...  163 us
    unnamed x3, local copies, waits for them, and re-layouts  6.81 us

profile of v3, /device:TPU:0, one launch (start us, length us, event | category | flops | bytes accessed | tf_op | source)
XLA Modules:
  0.0 169.9 jit_solution(5416472242288271359)
XLA Ops:
  0.0 2.2 %copy.15 = bf16[128,2816]{0,1:T(8,128)(2,1)} copy(bf16[128,2816]{1,0:T(8,128)(2,1)} %param.23) | data formatting | bytes 1441792 | tf_op args[9]
  2.2 2.3 %copy.16 = bf16[128,2816]{0,1:T(8,128)(2,1)} copy(bf16[128,2816]{1,0:T(8,128)(2,1)} %param.24) | data formatting | bytes 1441792 | tf_op args[10]
  4.5 163.1 %layer.1 = bf16[256,2048]{1,0:T(8,128)(2,1)} custom-call(bf16[512,1024]{1,0:T(8,128)(2,1)} %q_far.1, bf16[512,256]{1,0:T(8,128)(2,1)} %k_ref.1, bf16[512,256]{1,0:T(8,128)(2,1)} %v_ref.1, f32[16]{0:T(128)} %sink_ref.1, bf16[1024,2048]{1,0:T(8,128)(2,1)} %ow_far.1, bf16[256,2048]{1,0:T(8,128)(2,1)} %res_far.1, f32[1,2048]{1,0:T(1,128)} %bitcast.7, ...), custom_call_target="tpu_custom_call" | custom-call | tf_op jit(solution)/shard_map/layer/pallas_call | solution.py:776
  167.6 2.3 %copy.18 = bf16[256,2048]{1,0:T(8,128)(2,1)} copy(bf16[256,2048]{1,0:T(8,128)(2,1)} %layer.1) | data formatting | bytes 2097152

commit v4 on v3

--- a/solution.py
+++ b/solution.py
@@ -231,6 +231,7 @@
     edge_r,
     sum_s,
     sum_r,
+    raw_sem,
 ):
     sp, tp = lax.axis_index("sp"), lax.axis_index("tp")
     members = ring * TEAM
@@ -239,7 +240,7 @@
     length = q_ref.shape[0]
     share = length // 2
     units = gate_all.shape[0]
-    wide = gate_far.shape[1]
+    wide, deep = down_far.shape[1], gate_far.shape[0]
     last = ring - 2
     parts = unit_parts(units)
     cuts = ((0, 2), (2, 1), (3, 1))
@@ -247,6 +248,26 @@
 
     def peer(turn):
         return level * TEAM + team_peer(place, turn)
+
+    group = psnd.shape[2]
+    stacked_raw = psnd.shape[1] // deep
+
+    def raw_piece(m, i):
+        at = pl.ds(i % stacked_raw * deep, deep)
+        return psnd.at[2 * m + i // stacked_raw, at]
+
+    raws = [
+        [
+            pltpu.make_async_copy(
+                ref.at[:, pl.ds(i * group, group)], raw_piece(m, i), raw_sem.at[m, i]
+            )
+            for i in range(ref.shape[1] // group)
+        ]
+        for m, ref in enumerate((gate_far, value_far))
+    ]
+    for copies in raws:
+        for copy in copies:
+            copy.start()
 
     has_up, has_down = level < ring - 1, level > 0
     has_after, has_before = sp < members - 1, sp > 0
@@ -294,14 +315,29 @@
         for i, (ref, ext) in enumerate(((k_ref, k_ext), (v_ref, v_ext)))
     ]
 
-    fars = (gate_far, value_far, down_far)
     wholes = (gate_all, value_all, down_all)
 
     def span(m, start, size):
         return wholes[m].at[:, pl.ds(pl.multiple_of(start * wide, wide), size * wide)]
 
     def piece(m, member):
-        return fars[m].at[pl.ds(pl.multiple_of(member * units, units), units)]
+        if m == 2:
+            return down_far.at[pl.ds(pl.multiple_of(member * units, units), units)]
+        return hid.at[pl.ds(m * units, units), pl.ds(pl.multiple_of(member * wide, wide), wide)]
+
+    def turn_round(m):
+        for i, copy in enumerate(raws[m]):
+            copy.wait()
+            turned = raw_piece(m, i)[...].T
+            at = i * group
+            while at < (i + 1) * group:
+                member, first = at // units, at % units
+                size = min(units - first, (i + 1) * group - at)
+                start = at - i * group
+                hid[m * units + first : m * units + first + size, member * wide : member * wide + wide] = (
+                    turned[start : start + size]
+                )
+                at += size
 
     def can_send(side, step):
         return has_up & (level >= step) if side == 0 else has_down & (level + step < ring)
@@ -364,10 +400,15 @@
         for side in range(2):
             begin(first_copy(m, side, place, piece(m, place)), can_send(side, 0))
 
-    trades, locals_ = [], []
-    for m in range(3):
-        trades.append(
+    trades, locals_, early = {}, {}, []
+
+    def launch(m):
+        mark = len(sends)
+        if m < 2:
+            turn_round(m)
+        trades.update(
             {
+                m: {
                 turn: begin(
                     remote(
                         piece(m, team_peer(place, turn)),
@@ -378,12 +419,19 @@
                     )
                 )
                 for turn in (1, 2, 3)
+                }
             }
         )
-        own_first(m)
+        if m < 2:
+            own_first(m)
+            early.extend(sends[mark:])
+            del sends[mark:]
         copy = pltpu.make_async_copy(piece(m, place), span(m, sp, 1), local_sem.at[m])
         copy.start()
-        locals_.append(copy)
+        locals_[m] = copy
+
+    launch(0)
+    own_first(2)
     fetch_q = pltpu.make_async_copy(q_far, q_ref, local_sem.at[5])
     fetch_q.start()
     fetch_kv = [
@@ -441,6 +489,8 @@
                 taps[i, : ref.shape[0]] = ref[:, p * units : (p + 1) * units]
 
     first_rest(0)
+    launch(1)
+    launch(2)
     for copy in halos:
         arrive(copy, has_before)
     fetch_q.wait()
@@ -485,7 +535,7 @@
             return carry
 
         lax.fori_loop(0, length // WINDOW, block_step, 0)
-        if kv == 0:
+        if kv == 1:
             first_rest(1)
 
     columns = ow.shape[1]
@@ -588,6 +638,11 @@
     up(0, gate_up)
     down_rest()
     locals_[1].wait()
+    for there, copy in early:
+        if there is None:
+            copy.wait_send()
+        else:
+            pl.when(there)(copy.wait_send)
     reach = gate_taps.shape[0] - 1
     conv_rows = 64
     per = share // conv_rows
@@ -827,6 +882,7 @@
             dma(()),
             dma((5, jobs)),
             dma((5, jobs)),
+            dma((2, local_units // group_cols)),
         ],
         compiler_params=pltpu.CompilerParams(
             collective_id=0, has_side_effects=True, vmem_limit_bytes=VMEM_BYTES
@@ -842,8 +898,8 @@
         gain_attn[None],
         gain_before[None],
         gain_after[None],
-        gate_weight.T,
-        value_weight.T,
+        gate_weight,
+        value_weight,
         down_weight,
         gate_taps,
         value_taps,

time: 170 us -> 165 us (0.971)
  local copies, waits for them, and re-layouts: 6.81 us -> 2.3 us
    unnamed x3 -> x1, local copies, waits for them, and re-layouts: 6.81 us -> 2.3 us
where the time goes in v4:
time: 165 us
  Pallas kernels  163 us (99%)
  local copies, waits for them, and re-layouts  2.3 us (1%)
    pallas_call x1, Pallas kernels, on_device_team(): pl.pallas_call(functools.partial(layer_kernel, ring), out_shape=jax.Shape...  163 us

profile of v4, /device:TPU:0, one launch (start us, length us, event | category | flops | bytes accessed | tf_op | source)
XLA Modules:
  0.0 165.0 jit_solution(16519842821498512473)
XLA Ops:
  0.0 162.7 %layer.1 = bf16[256,2048]{1,0:T(8,128)(2,1)} custom-call(bf16[512,1024]{1,0:T(8,128)(2,1)} %q_far.1, bf16[512,256]{1,0:T(8,128)(2,1)} %k_ref.1, bf16[512,256]{1,0:T(8,128)(2,1)} %v_ref.1, f32[16]{0:T(128)} %sink_ref.1, bf16[1024,2048]{1,0:T(8,128)(2,1)} %ow_far.1, bf16[256,2048]{1,0:T(8,128)(2,1)} %res_far.1, f32[1,2048]{1,0:T(1,128)} %bitcast.3, ...), custom_call_target="tpu_custom_call" | custom-call | tf_op jit(solution)/shard_map/layer/pallas_call | solution.py:831
  162.7 2.3 %copy.16 = bf16[256,2048]{1,0:T(8,128)(2,1)} copy(bf16[256,2048]{1,0:T(8,128)(2,1)} %layer.1) | data formatting | bytes 2097152

commit v5 on v4

--- a/solution.py
+++ b/solution.py
@@ -488,8 +488,8 @@
             for i, ref in enumerate((gate_taps, value_taps)):
                 taps[i, : ref.shape[0]] = ref[:, p * units : (p + 1) * units]
 
+    launch(1)
     first_rest(0)
-    launch(1)
     launch(2)
     for copy in halos:
         arrive(copy, has_before)
@@ -635,8 +635,8 @@
 
     receive(0, last)
     locals_[0].wait()
+    down_rest()
     up(0, gate_up)
-    down_rest()
     locals_[1].wait()
     for there, copy in early:
         if there is None:

time: 165 us -> 165 us (level)
  Pallas kernels: 163 us -> 161 us
where the time goes in v5:
time: 165 us; the launch traced here: 164 us
  Pallas kernels  161 us (98%)
  local copies, waits for them, and re-layouts  2.3 us (1%)
    pallas_call x1, Pallas kernels, on_device_team(): pl.pallas_call(functools.partial(layer_kernel, ring), out_shape=jax.Shape...  161 us

profile of v5, /device:TPU:0, one launch (start us, length us, event | category | flops | bytes accessed | tf_op | source)
XLA Modules:
  0.0 163.7 jit_solution(17957206018123817725)
XLA Ops:
  0.0 161.3 %layer.1 = bf16[256,2048]{1,0:T(8,128)(2,1)} custom-call(bf16[512,1024]{1,0:T(8,128)(2,1)} %q_far.1, bf16[512,256]{1,0:T(8,128)(2,1)} %k_ref.1, bf16[512,256]{1,0:T(8,128)(2,1)} %v_ref.1, f32[16]{0:T(128)} %sink_ref.1, bf16[1024,2048]{1,0:T(8,128)(2,1)} %ow_far.1, bf16[256,2048]{1,0:T(8,128)(2,1)} %res_far.1, f32[1,2048]{1,0:T(1,128)} %bitcast.3, ...), custom_call_target="tpu_custom_call" | custom-call | tf_op jit(solution)/shard_map/layer/pallas_call | solution.py:831
  161.4 2.3 %copy.16 = bf16[256,2048]{1,0:T(8,128)(2,1)} copy(bf16[256,2048]{1,0:T(8,128)(2,1)} %layer.1) | data formatting | bytes 2097152
